TPU v7x, 32 devices: a whole 2x2x4 slice. The times are simulated.
32 devices in a mesh: grp: 2 (over y), sp: 4 (over z), fs: 2 (over x), tp: 2 (over core).
Axes of the slice: x: 2, y: 2, z: 4, core: 2. Of those that a mesh axis runs over, the one named last changes fastest.
Arguments:
- tokens: bfloat16 [2, 6144, 2048], P('fs', ('grp', 'sp'), 'tp'), parts along dimension 1, may hold values from -12 to 12
- norm_gain: float32 [2048], replicated, may hold values from 0.1 to 1.9
- query_weight: bfloat16 [2048, 16, 64], P(None, 'tp'), may hold values from -3 to 3
- key_weight: bfloat16 [2048, 4, 64], P(None, 'tp'), may hold values from -3 to 3
- value_weight: bfloat16 [2048, 4, 64], P(None, 'tp'), may hold values from -0.125 to 0.125
- sink_logit: float32 [16], P('tp'), may hold values from 1 to 6
- pool_weight: bfloat16 [2048, 4, 256], P(None, None, 'tp'), may hold values from -0.125 to 0.125
- attn_out_weight: bfloat16 [16, 64, 2048], P('tp'), may hold values from -0.5 to 0.5
- pool_out_weight: bfloat16 [4, 256, 2048], P(None, 'tp'), may hold values from -0.1875 to 0.1875
Outputs:
- mixed: bfloat16 [2, 6144, 2048], P('fs', ('grp', 'sp', 'tp')), parts along dimension 1
There are 2 independent parts, one for each index of `grp`. A program takes and returns all parts, laid end to end along the dimension named above; an argument that names none is the same for every part. Nothing has to cross between parts.
All inputs are finite; a program needn't handle non-finite values.
Results may differ from a plain program's by a relative error of at most 0.0095.
The roundings to bfloat16 on the way count: a program that leaves them out, or rounds other values in their place, can miss the bound.
Values may be sent and summed in bfloat16 or wider, within the bound.
A program may use at most 128 MiB of HBM per device.

v0:
```python
import jax
import jax.numpy as jnp
from jax import lax
from jax.sharding import PartitionSpec as P

WINDOW = 128


def from_behind(value, axis, steps):
    count = lax.axis_size(axis)
    first, last = (max(0, -steps), min(count, count - steps))
    return lax.ppermute(value, axis, [(source, source + steps) for source in range(first, last)])


def rms_norm(rows, gain):
    values = rows.astype(jnp.float32)
    scale = lax.rsqrt(jnp.mean(values * values, axis=-1, keepdims=True) + 1e-06)
    return (values * scale * gain).astype(jnp.bfloat16)


def attend(query, key, value, key_tail, value_tail, sinks, offset):
    rows = query.shape[0]
    local_kv = key_tail.shape[1]
    head_dim = key_tail.shape[2]
    group = query.shape[1] // (local_kv * head_dim)
    blocks = rows // WINDOW
    qb = query.reshape(blocks, WINDOW, local_kv, group, head_dim)

    def banded(tensor, tail):
        tb = tensor.reshape(blocks, WINDOW, local_kv, head_dim)
        whole = jnp.concatenate([tail, tensor.reshape(rows, local_kv, head_dim)], axis=0)
        before = whole[:rows].reshape(blocks, WINDOW, local_kv, head_dim)
        return jnp.concatenate([before, tb], axis=1)

    kw = banded(key, key_tail)
    vw = banded(value, value_tail)
    qi = jnp.arange(WINDOW, dtype=jnp.int32)[:, None]
    kj = jnp.arange(2 * WINDOW, dtype=jnp.int32)[None, :]
    dist = WINDOW + qi - kj
    inside = (dist >= 0) & (dist < WINDOW)
    key_pos = (
        offset + jnp.arange(blocks, dtype=jnp.int32)[:, None, None] * WINDOW - WINDOW + kj[None]
    )
    mask = inside[None] & (key_pos >= 0)
    scores = jnp.einsum(
        "nqhgd,nkhd->nhgqk", qb, kw, preferred_element_type=jnp.float32
    ) * head_dim ** (-0.5)
    scores = jnp.where(mask[:, None, None], scores, -jnp.inf)
    sink = sinks.reshape(1, local_kv, group, 1, 1)
    top = jnp.maximum(jnp.max(scores, axis=-1, keepdims=True), sink)
    expo = jnp.exp(scores - top)
    total = jnp.sum(expo, axis=-1, keepdims=True) + jnp.exp(sink - top)
    weight = (expo / total).astype(jnp.bfloat16)
    out = jnp.einsum("nhgqk,nkhd->nqhgd", weight, vw, preferred_element_type=jnp.float32)
    return out.reshape(rows, -1).astype(jnp.bfloat16)


def shards(
    tokens,
    norm_gain,
    query_weight,
    key_weight,
    value_weight,
    sink_logit,
    pool_weight,
    attn_out_weight,
    pool_out_weight,
):
    whole = lax.all_gather(tokens, "tp", axis=2, tiled=True)[0]
    rows = whole.shape[0]
    width = whole.shape[1]
    local_kv = key_weight.shape[1]
    head_dim = key_weight.shape[2]
    channels = pool_weight.shape[2]
    normed = rms_norm(whole, norm_gain)
    query = jnp.dot(
        normed, query_weight.reshape(width, -1), preferred_element_type=jnp.float32
    ).astype(jnp.bfloat16)
    key = jnp.dot(normed, key_weight.reshape(width, -1), preferred_element_type=jnp.float32).astype(
        jnp.bfloat16
    )
    value = jnp.dot(
        normed, value_weight.reshape(width, -1), preferred_element_type=jnp.float32
    ).astype(jnp.bfloat16)
    pooled_in = jnp.dot(
        normed, pool_weight.reshape(width, -1), preferred_element_type=jnp.float32
    ).astype(jnp.bfloat16)
    pool_rows = pooled_in.reshape(rows, 4, channels)
    key_rows = key.reshape(rows, local_kv, head_dim)
    value_rows = value.reshape(rows, local_kv, head_dim)
    key_tail, value_tail, pool_tail = from_behind(
        (key_rows[rows - WINDOW :], value_rows[rows - WINDOW :], pool_rows[rows - WINDOW :]),
        "sp",
        1,
    )
    offset = lax.axis_index("sp") * rows
    attended = attend(query, key, value, key_tail, value_tail, sink_logit, offset)
    prefix_total = jnp.sum(pool_rows[:, 3].astype(jnp.float32), axis=0)
    totals = lax.all_gather(prefix_total[None], "sp", axis=0, tiled=True)
    below = jnp.arange(totals.shape[0], dtype=jnp.int32) < lax.axis_index("sp")
    carried = jnp.sum(jnp.where(below[:, None], totals, 0.0), axis=0)
    reaches = jnp.array([2.0, 4.0, 16.0, 1000000000.0], jnp.float32)
    ext = jnp.concatenate([pool_tail, pool_rows], axis=0)
    position = jnp.arange(rows, dtype=jnp.int32)[:, None]
    source = jnp.arange(rows + WINDOW, dtype=jnp.int32)[None, :]
    gap = (position + WINDOW - source).astype(jnp.float32)
    group_ids = jnp.arange(4, dtype=jnp.int32)[:, None, None]
    band = (
        (gap[None] >= 0.0)
        & (gap[None] < reaches[:, None, None])
        & ((group_ids < 3) | (source[None] >= WINDOW))
    )
    sums = jnp.einsum(
        "gij,jgc->igc", band.astype(jnp.bfloat16), ext, preferred_element_type=jnp.float32
    )
    carry_rows = jnp.concatenate([jnp.zeros((3, channels), jnp.float32), carried[None]], axis=0)
    sums = sums + carry_rows[None]
    count = (offset + jnp.arange(1, rows + 1, dtype=jnp.int32)).astype(jnp.float32)
    denom = jnp.minimum(count[:, None], reaches[None, :])[:, :, None]
    pooled = (
        (sums / denom - pool_rows.astype(jnp.float32))
        .astype(jnp.bfloat16)
        .reshape(rows, 4 * channels)
    )
    attn_rows = attn_out_weight.reshape(-1, width)
    pool_weight_rows = pool_out_weight.reshape(-1, width)
    part_sum = jnp.dot(attended, attn_rows, preferred_element_type=jnp.float32)
    result = lax.psum_scatter(
        (part_sum + jnp.dot(pooled, pool_weight_rows, preferred_element_type=jnp.float32)).astype(
            jnp.bfloat16
        ),
        "tp",
        scatter_dimension=0,
        tiled=True,
    )
    return result[None]


def solution(mesh):
    in_specs = (
        P("fs", ("grp", "sp"), "tp"),
        P(),
        P(None, "tp", None),
        P(None, "tp", None),
        P(None, "tp", None),
        P("tp"),
        P(None, None, "tp"),
        P("tp", None, None),
        P(None, "tp", None),
    )
    out_specs = P("fs", ("grp", "sp", "tp"), None)
    return jax.shard_map(shards, mesh=mesh, in_specs=in_specs, out_specs=out_specs, check_vma=False)
```

profile of v0, /device:TPU:1, one launch (start us, length us, event | category | flops | bytes accessed | tf_op | source)
XLA Modules:
  0.0 103.7 jit_solution(3450044622372322319)
XLA Ops:
  6.5 0.0 copy-start
  6.5 0.0 all-gather.4.cloned.1.call-start
  6.5 0.7 all-gather.4.cloned.1.call-update
  7.3 0.0 reduce-scatter.2.cloned.1.call-start
  7.3 0.7 max.18
  8.1 0.1 add_compare_fusion
  8.2 0.7 broadcast_or_fusion
  8.8 0.7 broadcast_minimum_fusion
  9.6 0.3 broadcast_and_fusion
  9.9 0.0 copy-start.10
  9.9 1.5 %broadcast_compare_fusion = pred[768,896]{1,0:T(8,128)(4,1)} fusion(s32[768]{0:T(1024)S(1)} %iota_add_fusion), kind=kLoop, calls=%fused_computation.34 | loop fusion | flops 2064384 | bytes 691200 | tf_op jit(solution)/shard_map/ge | solution.py:109
  11.4 1.8 %subtract_convert_fusion = f32[768,896]{1,0:T(8,128)} fusion(s32[768]{0:T(1024)S(1)} %iota_add_fusion), kind=kLoop, calls=%fused_computation.22 | loop fusion | flops 1376256 | bytes 2755584 | tf_op jit(solution)/shard_map/convert_element_type | solution.py:106
  13.1 10.4 %all-gather.4.cloned.1.call-done = bf16[1,768,2048]{2,1,0:T(8,128)(2,1)} async-done(((bf16[1,768,1024]{2,1,0:T(8,128)(2,1)}), bf16[1,768,2048]{2,1,0:T(8,128)(2,1)}) %all-gather.4.cloned.1.call-update) | async-done | bytes 3145744 | tf_op jit(solution)/shard_map/all_gather | solution.py:69
  23.5 0.0 copy-start.1
  23.5 2.7 %fusion.4 = f32[768]{0:T(1024)S(1)} fusion(bf16[1,768,2048]{2,1,0:T(8,128)(2,1)} %all-gather.4.cloned.1.call-done), kind=kLoop, calls=%fused_computation.6 | loop fusion | flops 4717824 | bytes 3148800 | tf_op jit(solution)/shard_map/reduce_sum | solution.py:17
  26.2 0.0 copy-done.10
  26.2 0.1 copy-done.1
  26.3 2.3 %convolution_convert_fusion.2 = bf16[768,128]{0,1:T(8,128)(2,1)S(1)} fusion(bf16[2048,128]{0,1:T(8,128)(2,1)} %bitcast.105, bf16[1,768,2048]{2,1,0:T(8,128)(2,1)S(1)} %copy-done.1, f32[2048]{0:T(1024)S(1)} %copy-done.10, f32[768]{0:T(1024)S(1)} %add_rsqrt_fusion), kind=kOutput, calls=%fused_computation.37 | convolution fusion | flops 409042944 | bytes 3877888 | tf_op jit(solution)/shard_map/dot_general | solution.py:82
  28.7 0.2 reshape.317
  28.9 0.0 copy-start.2
  28.9 0.0 copy-start.8
  28.9 3.4 %convolution_convert_fusion.1 = bf16[768,128]{0,1:T(8,128)(2,1)S(1)} fusion(bf16[2048,128]{0,1:T(8,128)(2,1)} %bitcast.106, bf16[1,768,2048]{2,1,0:T(8,128)(2,1)} %all-gather.4.cloned.1.call-done, f32[2048]{0:T(1024)S(1)} %copy-done.10, f32[768]{0:T(1024)S(1)} %add_rsqrt_fusion), kind=kOutput, calls=%fused_computation.36 | convolution fusion | flops 409042944 | bytes 3877888 | tf_op jit(solution)/shard_map/dot_general | solution.py:79
  32.3 4.1 %collective-permute-start.1 = (bf16[128,2,64]{0,2,1:T(8,128)(2,1)S(1)}, bf16[128,2,64]{0,2,1:T(8,128)(2,1)}, u32[]{:S(2)}, u32[]{:S(2)}) collective-permute-start(bf16[128,2,64]{0,2,1:T(8,128)(2,1)S(1)} %bitcast.99), channel_id=1, source_target_pairs={{0,4},{4,8},{8,12},{1,5},{5,9},{9,13},{2,6},{6,10},{10,14},{3,7},{... | collective-permute-start | bytes 98312 | tf_op jit(solution)/shard_map/ppermute | solution.py:12
  36.4 3.1 %collective-permute-start = (bf16[128,2,64]{0,2,1:T(8,128)(2,1)S(1)}, bf16[128,2,64]{0,2,1:T(8,128)(2,1)}, u32[]{:S(2)}, u32[]{:S(2)}) collective-permute-start(bf16[128,2,64]{0,2,1:T(8,128)(2,1)S(1)} %bitcast.98), channel_id=1, source_target_pairs={{0,4},{4,8},{8,12},{1,5},{5,9},{9,13},{2,6},{6,10},{10,14},{3,7},{... | collective-permute-start | bytes 98312 | tf_op jit(solution)/shard_map/ppermute | solution.py:12
  39.5 0.0 copy-done.2
  39.5 0.0 copy-done.8
  39.6 0.0 copy-start.9
  39.6 2.0 %fusion.25 = bf16[768,512]{0,1:T(8,128)(2,1)S(1)} fusion(bf16[256,8,4,128]{3,2,1,0:T(4,128)(2,1)S(1)} %bitcast.103, bf16[1,768,2048]{2,1,0:T(8,128)(2,1)S(1)} %copy-done.2, f32[2048]{0:T(1024)S(1)} %copy-done.10, f32[768]{0:T(1024)S(1)} %add_rsqrt_fusion), kind=kOutput, calls=%fused_computation.31 | convolution fusion | flops 1617297408 | bytes 6040576 | tf_op jit(solution)/shard_map/dot_general | solution.py:85
  41.6 0.0 copy-start.4
  41.6 0.1 convert_reduce_fusion
  41.7 6.4 %all-gather.1 = f32[4,1,128]{2,1,0:T(1,128)S(1)} all-gather(f32[1,1,128]{2,1,0:T(1,128)S(1)} %bitcast.101), channel_id=2, replica_groups=mesh['grp'=2,'sp'=4,'fs'=2,'tp'=2] {'sp'}, dimensions={0}, use_global_device_ids=true | all-gather | bytes 2560 | tf_op jit(solution)/shard_map/all_gather | solution.py:99
  48.2 3.4 %collective-permute-start.2 = (bf16[128,4,128]{0,2,1:T(8,128)(2,1)S(1)}, bf16[128,4,128]{0,2,1:T(8,128)(2,1)}, u32[]{:S(2)}, u32[]{:S(2)}) collective-permute-start(bf16[128,4,128]{0,2,1:T(8,128)(2,1)S(1)} %bitcast.97), channel_id=1, source_target_pairs={{0,4},{4,8},{8,12},{1,5},{5,9},{9,13},{2,6},{6,10},{10,14},{3,7},{... | collective-permute-start | bytes 393224 | tf_op jit(solution)/shard_map/ppermute | solution.py:12
  51.6 0.0 copy-done.9
  51.6 2.7 %convolution_convert_fusion = bf16[768,512]{1,0:T(8,128)(2,1)} fusion(bf16[2048,512]{0,1:T(8,128)(2,1)S(1)} %bitcast.104, bf16[1,768,2048]{2,1,0:T(8,128)(2,1)S(1)} %copy-done.2, f32[2048]{0:T(1024)S(1)} %copy-done.10, f32[768]{0:T(1024)S(1)} %add_rsqrt_fusion), kind=kOutput, calls=%fused_computation.32 | convolution fusion | flops 1617297408 | bytes 6040576 | tf_op jit(solution)/shard_map/dot_general | solution.py:76
  54.3 0.0 copy-done.4
  54.3 0.7 select_reduce_fusion
  55.0 0.2 reshape.321
  55.2 3.6 %reshape.334 = bf16[6,128,2,4,64]{4,3,2,1,0:T(4,128)(2,1)} reshape(bf16[768,512]{1,0:T(8,128)(2,1)} %convolution_convert_fusion) | data formatting | bytes 1572864 | tf_op jit(solution)/shard_map/reshape | solution.py:27
  58.9 1.3 %concatenate.23 = f32[4,128]{1,0:T(4,128)} pad(f32[1,128]{1,0:T(1,128)} %bitcast.102, f32[]{:T(128)} %constant.14.clone.1), padding=3_0x0_0 | pad | bytes 2564 | tf_op jit(solution)/shard_map/concatenate | solution.py:116
  60.2 0.0 collective-permute-done.1
  60.2 0.8 copy_bitcast_fusion
  61.0 2.7 %fusion.13 = (f32[6,2,4,128]{3,2,1,0:T(4,128)S(1)}, f32[6,2,256,128,4]{3,2,4,1,0:T(8,128)S(1)}) fusion(pred[6,128,256]{1,2,0:T(8,128)(4,1)S(1)} %broadcast_and_fusion, bf16[6,128,2,4,64]{4,3,2,1,0:T(4,128)(2,1)} %reshape.334, bf16[6,128,2,64]{1,3,2,0:T(8,128)(2,1)S(1)} %copy.28, bf16[6,128,2,64]{1,3,2,0:T(8,128)(2,1)S(1)} %copy_bitcast_fusion), kind=kOutput, calls=%fused_computation.19 | convolution fusion | flops 206825472 | bytes 7692288 | tf_op jit(solution)/shard_map/nqhgd,nkhd->nhgqk/dot_general | solution.py:45
  63.6 0.1 broadcast_maximum_fusion
  63.7 1.7 %fusion.8 = f32[6,2,4,128]{3,2,1,0:T(4,128)S(1)} fusion(f32[6,2,256,128,4]{3,2,4,1,0:T(8,128)S(1)} %get-tuple-element.6, f32[6,2,4,128]{3,2,1,0:T(4,128)S(1)} %broadcast_maximum_fusion, pred[6,128,256]{1,2,0:T(8,128)(4,1)S(1)} %broadcast_and_fusion), kind=kLoop, calls=%fused_computation.14 | loop fusion | flops 6285312 | bytes 6537216 | tf_op jit(solution)/shard_map/reduce_sum | solution.py:52
  65.4 0.1 exponential_add_fusion
  65.5 0.0 collective-permute-done
  65.5 0.8 copy_bitcast_fusion.1
  66.3 1.7 %fusion.31 = bf16[6,128,2,4,64]{1,4,3,2,0:T(8,128)(2,1)S(1)} fusion(f32[6,2,256,128,4]{3,2,4,1,0:T(8,128)S(1)} %get-tuple-element.6, f32[6,2,4,128]{3,2,1,0:T(4,128)S(1)} %exponential_add_fusion, f32[6,2,4,128]{3,2,1,0:T(4,128)S(1)} %broadcast_maximum_fusion, pred[6,128,256]{1,2,0:T(8,128)(4,1)S(1)} %broadcast_and_fusion, ...), kind=kOutput, calls=%fused_computation.35 | convolution fusion | flops 210370560 | bytes 7716864 | tf_op jit(solution)/shard_map/nhgqk,nkhd->nqhgd/dot_general | solution.py:54
  68.0 0.6 copy.32
  68.6 0.0 copy-done
  68.6 0.0 copy-start.3
  68.6 0.0 copy-start.5
  68.6 0.0 copy-start.6
  68.6 0.0 copy-start.7
  68.6 4.5 %fusion.38 = f32[768,2048]{1,0:T(8,128)} fusion(bf16[512,2048]{1,0:T(8,128)(2,1)S(1)} %bitcast.91, bf16[64,8,6,128]{3,2,1,0:T(8,128)(2,1)S(1)} %bitcast.92), kind=kOutput, calls=%fused_computation.41 | convolution fusion | flops 1610612736 | bytes 9175040 | tf_op jit(solution)/shard_map/dot_general | solution.py:127
  73.1 0.0 collective-permute-done.2
  73.1 0.0 copy-done.3
  73.1 0.0 copy-done.5
  73.1 0.0 copy-done.6
  73.1 0.0 copy-done.7
  73.1 11.3 %fusion.7 = bf16[768,2048]{1,0:T(8,128)(2,1)} fusion(f32[768,2048]{1,0:T(8,128)} %fusion.38, bf16[4,128,2048]{2,1,0:T(8,128)(2,1)} %param.18, bf16[768,4,128]{0,2,1:T(8,128)(2,1)} %bitcast.96, f32[768,896]{1,0:T(8,128)} %subtract_convert_fusion, f32[4]{0:T(128)S(1)} %copy-done.7, pred[4,896]{1,0:T(4,128)(4,1)S(1)} %copy-done.5, ...), kind=kOutput, calls=%fused_computation.10 | convolution fusion | flops 2330460160 | bytes 15910416 | tf_op jit(solution)/shard_map/dot_general | solution.py:129
  84.5 0.0 reduce-scatter.2.cloned.1.call-update
  84.5 12.3 %reduce-scatter.2.cloned.1.call-done = bf16[384,2048]{1,0:T(8,128)(2,1)} async-done(((bf16[768,2048]{1,0:T(8,128)(2,1)}), bf16[384,2048]{1,0:T(8,128)(2,1)}) %reduce-scatter.2.cloned.1.call-update) | async-done | bytes 1572880 | tf_op jit(solution)/shard_map/reduce_scatter | solution.py:128
  (14 shorter events, 0.2 us)
Async XLA Ops:
  6.5 62.0 %copy-start = (bf16[8,64,2048]{2,1,0:T(8,128)(2,1)S(1)}, bf16[8,64,2048]{2,1,0:T(8,128)(2,1)}, u32[]{:S(2)}) copy-start(bf16[8,64,2048]{2,1,0:T(8,128)(2,1)} %param.17) | copy-start | bytes 6291460
  6.5 16.9 %all-gather.4.cloned.1.call-start = ((), (), s32[]{:S(2)}) async-start(), calls=%async_computation.1 | async-start | bytes 4718592 | tf_op jit(solution)/shard_map/all_gather | solution.py:69
  7.3 89.6 %reduce-scatter.2.cloned.1.call-start = ((), (), s32[]{:S(2)}) async-start(), calls=%async_computation.2 | async-start | bytes 4718592 | tf_op jit(solution)/shard_map/reduce_scatter | solution.py:128
  9.9 16.3 %copy-start.10 = (f32[2048]{0:T(1024)S(1)}, f32[2048]{0:T(1024)}, u32[]{:S(2)}) copy-start(f32[2048]{0:T(1024)} %param.11) | copy-start | bytes 24580
  23.5 2.8 %copy-start.1 = (bf16[1,768,2048]{2,1,0:T(8,128)(2,1)S(1)}, bf16[1,768,2048]{2,1,0:T(8,128)(2,1)}, u32[]{:S(2)}) copy-start(bf16[1,768,2048]{2,1,0:T(8,128)(2,1)} %all-gather.4.cloned.1.call-done) | copy-start | bytes 9437188
  28.9 10.6 %copy-start.2 = (bf16[1,768,2048]{2,1,0:T(8,128)(2,1)S(1)}, bf16[1,768,2048]{2,1,0:T(8,128)(2,1)}, u32[]{:S(2)}) copy-start(bf16[1,768,2048]{2,1,0:T(8,128)(2,1)} %all-gather.4.cloned.1.call-done) | copy-start | bytes 9437188
  28.9 10.6 %copy-start.8 = (bf16[2048,4,128]{2,1,0:T(4,128)(2,1)S(1)}, bf16[2048,4,128]{2,1,0:T(4,128)(2,1)}, u32[]{:S(2)}) copy-start(bf16[2048,4,128]{2,1,0:T(4,128)(2,1)} %param.16) | copy-start | bytes 6291460
  32.3 27.8 %collective-permute-start.1 = (bf16[128,2,64]{0,2,1:T(8,128)(2,1)S(1)}, bf16[128,2,64]{0,2,1:T(8,128)(2,1)}, u32[]{:S(2)}, u32[]{:S(2)}) collective-permute-start(bf16[128,2,64]{0,2,1:T(8,128)(2,1)S(1)} %bitcast.99), channel_id=1, source_target_pairs={{0,4},{4,8},{8,12},{1,5},{5,9},{9,13},{2,6},{6,10},{10,14},{3,7},{... | collective-permute-start | bytes 98312 | tf_op jit(solution)/shard_map/ppermute | solution.py:12
  36.4 29.1 %collective-permute-start = (bf16[128,2,64]{0,2,1:T(8,128)(2,1)S(1)}, bf16[128,2,64]{0,2,1:T(8,128)(2,1)}, u32[]{:S(2)}, u32[]{:S(2)}) collective-permute-start(bf16[128,2,64]{0,2,1:T(8,128)(2,1)S(1)} %bitcast.98), channel_id=1, source_target_pairs={{0,4},{4,8},{8,12},{1,5},{5,9},{9,13},{2,6},{6,10},{10,14},{3,7},{... | collective-permute-start | bytes 98312 | tf_op jit(solution)/shard_map/ppermute | solution.py:12
  39.6 12.0 %copy-start.9 = (bf16[2048,8,64]{0,2,1:T(8,128)(2,1)S(1)}, bf16[2048,8,64]{0,2,1:T(8,128)(2,1)}, u32[]{:S(2)}) copy-start(bf16[2048,8,64]{0,2,1:T(8,128)(2,1)} %param.12) | copy-start | bytes 6291460
  41.6 12.7 %copy-start.4 = (bf16[768,512]{0,1:T(8,128)(2,1)}, bf16[768,512]{0,1:T(8,128)(2,1)S(1)}, u32[]{:S(2)}) copy-start(bf16[768,512]{0,1:T(8,128)(2,1)S(1)} %fusion.25) | copy-start | bytes 2359300
  48.2 24.9 %collective-permute-start.2 = (bf16[128,4,128]{0,2,1:T(8,128)(2,1)S(1)}, bf16[128,4,128]{0,2,1:T(8,128)(2,1)}, u32[]{:S(2)}, u32[]{:S(2)}) collective-permute-start(bf16[128,4,128]{0,2,1:T(8,128)(2,1)S(1)} %bitcast.97), channel_id=1, source_target_pairs={{0,4},{4,8},{8,12},{1,5},{5,9},{9,13},{2,6},{6,10},{10,14},{3,7},{... | collective-permute-start | bytes 393224 | tf_op jit(solution)/shard_map/ppermute | solution.py:12
  68.6 4.5 %copy-start.3 = (pred[768,896]{1,0:T(8,128)(4,1)S(1)}, pred[768,896]{1,0:T(8,128)(4,1)}, u32[]{:S(2)}) copy-start(pred[768,896]{1,0:T(8,128)(4,1)} %broadcast_compare_fusion) | copy-start | bytes 2064388
  68.6 4.5 %copy-start.5 = (pred[4,896]{1,0:T(4,128)(4,1)S(1)}, pred[4,896]{1,0:T(4,128)(4,1)}, u32[]{:S(2)}) copy-start(pred[4,896]{1,0:T(4,128)(4,1)} %broadcast_or_fusion) | copy-start | bytes 10756
  68.6 4.5 %copy-start.6 = (f32[4,128]{1,0:T(4,128)S(1)}, f32[4,128]{1,0:T(4,128)}, u32[]{:S(2)}) copy-start(f32[4,128]{1,0:T(4,128)} %concatenate.23) | copy-start | bytes 6148
  68.6 4.5 %copy-start.7 = (f32[4]{0:T(128)S(1)}, f32[4]{0:T(128)}, u32[]{:S(2)}) copy-start(f32[4]{0:T(128)} %constant.13.clone) | copy-start | bytes 52
Sparse Core Ops, SparseCore 0:
  8.9 14.5 all-gather.3
  84.6 12.1 reduce-scatter.1
where the time goes:
time: 104 us
  matrix products  30.6 us (29%)
  waiting for transfers between devices  23.4 us (22%)
  between operations  13.7 us (13%)
  other arithmetic  12 us (12%)
  starting transfers between devices  10.6 us (10%)
  local copies, waits for them, and re-layouts  6.9 us (7%)
  blocking collectives  6.44 us (6%)
    reduce_scatter x1, waiting for transfers between devices, shards(): lax.psum_scatter((part_sum + jnp.dot(pooled, pool_weight_rows, preferred_...  12.3 us
    dot_general x1, matrix products, shards(): jnp.dot(pooled, pool_weight_rows, preferred_element_type=jnp.float32)  11.3 us
    ppermute x3, starting transfers between devices, from_behind(): lax.ppermute(value, axis, [(source, source + steps) for source in range(f...  10.6 us
    all_gather x1, waiting for transfers between devices, shards(): whole = lax.all_gather(tokens, 'tp', axis=2, tiled=True)[0]  10.4 us
    all_gather x1, blocking collectives, shards(): totals = lax.all_gather(prefix_total[None], 'sp', axis=0, tiled=True)  6.44 us
    dot_general x1, matrix products, shards(): part_sum = jnp.dot(attended, attn_rows, preferred_element_type=jnp.float32)  4.48 us
    reshape x1, local copies, waits for them, and re-layouts, attend(): qb = query.reshape(blocks, WINDOW, local_kv, group, head_dim)  3.63 us
    dot_general x1, matrix products, shards(): jnp.dot(normed, key_weight.reshape(width, -1), preferred_element_type=jnp...  3.39 us
  transfers between devices with their start and end apart: 5, of which 2 were waited for; matrix products, arithmetic and copies ran while one was open for 28% of the time, Pallas kernels for 0%

commit v1 on v0

v1 whole, which is shorter than its diff:
```python
import functools

import jax
import jax.numpy as jnp
from jax import lax
from jax.experimental import pallas as pl
from jax.experimental.pallas import tpu as pltpu
from jax.sharding import PartitionSpec as P

MESH = pl.DeviceIdType.MESH
WINDOW = 128
REACHES = (2, 4, 16)
TAIL = 16
CHUNK = 256
COLS = 512
F32 = jnp.float32
BF16 = jnp.bfloat16


def dot(a, b, dims=((1,), (0,))):
    return lax.dot_general(a, b, (dims, ((), ())), preferred_element_type=F32)


def kernel(
    n_sp,
    heads,
    local_kv,
    head_dim,
    tokens,
    gain,
    wq,
    wk,
    wv,
    sink,
    wp,
    wo,
    wpo,
    out,
    tok,
    normed,
    wqkv,
    wp_raw,
    wp_f32,
    wpool,
    wout,
    qt,
    kvt,
    ext,
    bands,
    block_sum,
    totals,
    act,
    sending,
    landing,
    result,
    w_sem,
    tok_sem,
    tok_send,
    tok_recv,
    halo_send,
    halo_recv,
    tot_send,
    tot_recv,
    out_send,
    out_recv,
    out_sem,
):
    me_sp = lax.axis_index("sp")
    me_tp = lax.axis_index("tp")
    other = 1 - me_tp
    rows, half_width = tokens.shape
    width = 2 * half_width
    q_rows = heads * head_dim
    kv_rows = local_kv * head_dim
    pool_cols = wpool.shape[1]
    channels = pool_cols // 4
    blocks = rows // WINDOW
    chunks = rows // CHUNK
    per_chunk = CHUNK // WINDOW
    half_rows = rows // 2
    half_blocks = blocks // 2
    tiles = width // COLS
    group = heads // local_kv

    barrier = pltpu.get_barrier_semaphore()
    pl.semaphore_signal(barrier, inc=1, device_id={"tp": other}, device_id_type=MESH)
    for step in range(1, n_sp):
        peer = lax.rem(me_sp + step, n_sp)
        pl.semaphore_signal(barrier, inc=1, device_id={"sp": peer}, device_id_type=MESH)

    load_wp = pltpu.make_async_copy(wp, wp_raw, w_sem.at[0])
    load_wp.start()

    def local_tokens(c):
        at = pl.ds(pl.multiple_of(c * CHUNK, CHUNK), CHUNK)
        return pltpu.make_async_copy(tokens.at[at, :], tok.at[me_tp, at, :], tok_sem.at[c])

    def remote_tokens(c):
        at = pl.ds(pl.multiple_of(c * CHUNK, CHUNK), CHUNK)
        return pltpu.make_async_remote_copy(
            src_ref=tokens.at[at, :],
            dst_ref=tok.at[me_tp, at, :],
            send_sem=tok_send.at[c],
            recv_sem=tok_recv.at[c],
            device_id={"tp": other},
            device_id_type=MESH,
        )

    for c in reversed(range(chunks)):
        local_tokens(c).start()
    loads = [
        pltpu.make_async_copy(wq, wqkv.at[pl.ds(0, q_rows), :], w_sem.at[1]),
        pltpu.make_async_copy(wk, wqkv.at[pl.ds(q_rows, kv_rows), :], w_sem.at[2]),
        pltpu.make_async_copy(wv, wqkv.at[pl.ds(q_rows + kv_rows, kv_rows), :], w_sem.at[3]),
    ]
    load_out = [
        pltpu.make_async_copy(wo, wout.at[pl.ds(0, q_rows), :], w_sem.at[4]),
        pltpu.make_async_copy(wpo, wout.at[pl.ds(q_rows, pool_cols), :], w_sem.at[5]),
    ]
    for load in loads:
        load.start()

    target = lax.broadcasted_iota(jnp.int32, (WINDOW, 2 * WINDOW), 0) + WINDOW
    source = lax.broadcasted_iota(jnp.int32, (WINDOW, 2 * WINDOW), 1)
    gap = target - source
    for g, reach in enumerate(REACHES):
        bands[g] = jnp.where((gap >= 0) & (gap < reach), 1.0, 0.0).astype(BF16)
    bands[3] = jnp.where((gap >= 0) & (gap < WINDOW) & (source >= WINDOW), 1.0, 0.0).astype(BF16)
    ext[pl.ds(0, WINDOW - TAIL), :] = jnp.zeros((WINDOW - TAIL, pool_cols), BF16)

    @pl.when(me_sp == 0)
    def _():
        ext[pl.ds(WINDOW - TAIL, TAIL), :] = jnp.zeros((TAIL, pool_cols), BF16)
        kvt[0] = jnp.zeros((2 * kv_rows, WINDOW), BF16)

    pl.semaphore_wait(barrier, n_sp)
    for c in reversed(range(chunks)):
        remote_tokens(c).start()
    for load in load_out:
        load.start()

    load_wp.wait()
    part = wp_f32.shape[0]

    def regroup(i, carry):
        wp_f32[...] = wp_raw[pl.ds(pl.multiple_of(i * part, part), part), :].astype(F32)
        at = pl.ds(pl.multiple_of(i * (part // 4), part // 4), part // 4)
        for g in range(4):
            wpool[at, pl.ds(g * channels, channels)] = wp_f32[
                pl.ds(g, part // 4, stride=4), :
            ].astype(BF16)
        return carry

    lax.fori_loop(0, wp_raw.shape[0] // part, regroup, 0)
    for load in loads:
        load.wait()

    halo_kv = pltpu.make_async_remote_copy(
        src_ref=kvt.at[blocks],
        dst_ref=kvt.at[0],
        send_sem=halo_send.at[0],
        recv_sem=halo_recv.at[0],
        device_id={"sp": lax.rem(me_sp + 1, n_sp)},
        device_id_type=MESH,
    )
    halo_pool = pltpu.make_async_remote_copy(
        src_ref=ext.at[pl.ds(WINDOW + rows - TAIL, TAIL), :],
        dst_ref=ext.at[pl.ds(WINDOW - TAIL, TAIL), :],
        send_sem=halo_send.at[1],
        recv_sem=halo_recv.at[1],
        device_id={"sp": lax.rem(me_sp + 1, n_sp)},
        device_id_type=MESH,
    )

    scale = head_dim ** (-0.5)

    def project(i, carry):
        c = chunks - 1 - i
        local_tokens(c).wait()
        remote_tokens(c).wait_recv()
        at = pl.ds(pl.multiple_of(c * CHUNK, CHUNK), CHUNK)
        low = tok[0, at, :].astype(F32)
        high = tok[1, at, :].astype(F32)
        square = jnp.sum(low * low, axis=1, keepdims=True)
        square = square + jnp.sum(high * high, axis=1, keepdims=True)
        inv = lax.rsqrt(square * (1.0 / width) + 1e-06)
        normed[:, pl.ds(0, half_width)] = (low * inv * gain[:, pl.ds(0, half_width)]).astype(BF16)
        normed[:, pl.ds(half_width, half_width)] = (
            high * inv * gain[:, pl.ds(half_width, half_width)]
        ).astype(BF16)

        @pl.when((i == 1) & (me_sp < n_sp - 1))
        def _():
            halo_kv.start()
            halo_pool.start()

        pooled_in = dot(normed[...], wpool[...]).astype(BF16)
        ext[pl.ds(pl.multiple_of(WINDOW + c * CHUNK, WINDOW), CHUNK), :] = pooled_in
        last = pooled_in[:, 3 * channels :].astype(F32)
        for j in range(per_chunk):
            summed = jnp.sum(last[j * WINDOW : (j + 1) * WINDOW], axis=0, keepdims=True)
            block_sum[c * per_chunk + j] = jnp.broadcast_to(summed, (8, channels))
        qkv = dot(wqkv[...], normed[...], ((1,), (1,)))
        for j in range(per_chunk):
            b = c * per_chunk + j
            piece = qkv[:, j * WINDOW : (j + 1) * WINDOW]
            qt[b] = (piece[:q_rows] * scale).astype(BF16)
            kvt[b + 1] = piece[q_rows:].astype(BF16)
        return carry

    lax.fori_loop(0, chunks, project, 0)

    all_rows = block_sum[0]
    for b in range(1, blocks):
        all_rows = all_rows + block_sum[b]
    totals[me_sp] = all_rows
    sends = []
    for step in range(1, n_sp):
        peer = lax.rem(me_sp + step, n_sp)
        sends.append(
            pltpu.make_async_remote_copy(
                src_ref=totals.at[me_sp],
                dst_ref=totals.at[me_sp],
                send_sem=tot_send.at[step],
                recv_sem=tot_recv.at[step],
                device_id={"sp": peer},
                device_id_type=MESH,
            )
        )

    key_at = lax.broadcasted_iota(jnp.int32, (WINDOW, group * WINDOW), 0)
    query_at = lax.rem(
        lax.broadcasted_iota(jnp.int32, (WINDOW, group * WINDOW), 1), jnp.int32(WINDOW)
    )
    own_key = key_at <= query_at

    def attend(b, slot):
        bias = jnp.where((b == 0) & (me_sp == 0), -jnp.inf, 0.0).astype(F32)
        parts = []
        for h in range(local_kv):
            q = jnp.concatenate(
                [
                    qt[b, pl.ds((h * group + g) * head_dim, head_dim), :]
                    for g in range(group)
                ],
                axis=1,
            )
            s = jnp.concatenate(
                [jnp.full((1, WINDOW), sink[h * group + g], F32) for g in range(group)], axis=1
            )
            k_at = pl.ds(h * head_dim, head_dim)
            v_at = pl.ds(kv_rows + h * head_dim, head_dim)
            before = dot(kvt[b, k_at, :], q, ((0,), (0,))) + bias
            own = dot(kvt[b + 1, k_at, :], q, ((0,), (0,)))
            score = jnp.where(own_key, own, before)
            top = jnp.maximum(jnp.max(score, axis=0, keepdims=True), s)
            expo = jnp.exp(score - top)
            total = jnp.sum(expo, axis=0, keepdims=True) + jnp.exp(s - top)
            weight = expo * (1.0 / total)
            w_before = jnp.where(own_key, 0.0, weight).astype(BF16)
            w_own = jnp.where(own_key, weight, 0.0).astype(BF16)
            gathered = dot(kvt[b, v_at, :], w_before) + dot(kvt[b + 1, v_at, :], w_own)
            parts += [gathered[:, g * WINDOW : (g + 1) * WINDOW] for g in range(group)]
        attended = jnp.concatenate(parts, axis=0)
        act[pl.ds(pl.multiple_of(slot * WINDOW, WINDOW), WINDOW), pl.ds(0, q_rows)] = (
            attended.T.astype(BF16)
        )

    def pool(b, slot, carried):
        start = pl.multiple_of(b * WINDOW, WINDOW)
        position = me_sp * rows + b * WINDOW + 1
        count = (lax.broadcasted_iota(jnp.int32, (WINDOW, channels), 0) + position).astype(F32)
        at = pl.ds(pl.multiple_of(slot * WINDOW, WINDOW), WINDOW)
        for g in range(4):
            col = pl.ds(g * channels, channels)
            own = ext[pl.ds(start + WINDOW, WINDOW), col]
            if g < 3:
                sums = dot(bands[g], ext[pl.ds(start, 2 * WINDOW), col])
                denom = jnp.minimum(count, float(REACHES[g]))
            else:
                base = carried
                for earlier in range(blocks):
                    base = base + jnp.where(earlier < b, block_sum[earlier], 0.0)
                sums = dot(bands[3, :, pl.ds(WINDOW, WINDOW)], own) + base[:1]
                denom = count
            pooled = sums * (1.0 / denom) - own.astype(F32)
            act[at, pl.ds(q_rows + g * channels, channels)] = pooled.astype(BF16)

    for send in sends:
        send.start()

    @pl.when(me_sp > 0)
    def _():
        halo_kv.wait_recv()
        halo_pool.wait_recv()

    def attend_half(first):
        def one(i, carry):
            attend(first + i, i)
            return carry

        lax.fori_loop(0, half_blocks, one, 0)

    def pool_half(first, carried):
        def one(i, carry):
            pool(first + i, i, carried)
            return carry

        lax.fori_loop(0, half_blocks, one, 0)

    first = other * half_blocks
    attend_half(first)
    for send in sends:
        send.wait()
    carried = jnp.zeros((8, channels), F32)
    for index in range(n_sp):
        carried = carried + jnp.where(index < me_sp, totals[index], 0.0)
    pool_half(first, carried)
    for load in load_out:
        load.wait()

    def partial_send(t):
        return pltpu.make_async_remote_copy(
            src_ref=sending.at[t],
            dst_ref=landing.at[t],
            send_sem=out_send.at[t],
            recv_sem=out_recv.at[t],
            device_id={"tp": other},
            device_id_type=MESH,
        )

    def columns(t):
        return pl.ds(pl.multiple_of(t * COLS, COLS), COLS)

    def give(t, carry):
        sending[t] = dot(act[...], wout[:, columns(t)]).astype(BF16)
        partial_send(t).start()
        return carry

    lax.fori_loop(0, tiles, give, 0)

    first = me_tp * half_blocks
    attend_half(first)
    pool_half(first, carried)

    def store(t):
        return pltpu.make_async_copy(result.at[t], out.at[:, columns(t)], out_sem.at[t])

    def keep(t, carry):
        partial_send(t).wait_recv()
        mine = dot(act[...], wout[:, columns(t)])
        result[t] = (mine + landing[t].astype(F32)).astype(BF16)
        store(t).start()
        return carry

    lax.fori_loop(0, tiles, keep, 0)
    for t in range(tiles):
        store(t).wait()
        partial_send(t).wait_send()
    for c in range(chunks):
        remote_tokens(c).wait_send()

    @pl.when(me_sp < n_sp - 1)
    def _():
        halo_kv.wait_send()
        halo_pool.wait_send()


def shards(n_sp, tokens, gain, wq, wk, wv, sink, wp, wo, wpo):
    rows, half_width = tokens.shape[1:]
    width = 2 * half_width
    heads, head_dim = wq.shape[1:]
    local_kv = wk.shape[1]
    channels = wp.shape[2]
    q_rows, kv_rows = (heads * head_dim, local_kv * head_dim)
    pool_cols = 4 * channels
    blocks = rows // WINDOW
    tiles = width // COLS
    chunks = rows // CHUNK
    dma = pltpu.SemaphoreType.DMA
    flat = lambda w: jnp.transpose(w, (1, 2, 0)).reshape(-1, width)
    hbm = pl.BlockSpec(memory_space=pl.ANY)
    vmem = pl.BlockSpec(memory_space=pltpu.VMEM)
    smem = pl.BlockSpec(memory_space=pltpu.SMEM)
    result = pl.pallas_call(
        functools.partial(kernel, n_sp, heads, local_kv, head_dim),
        out_shape=jax.ShapeDtypeStruct((rows // 2, width), BF16),
        in_specs=[hbm, vmem, hbm, hbm, hbm, smem, hbm, hbm, hbm],
        out_specs=hbm,
        scratch_shapes=[
            pltpu.VMEM((2, rows, half_width), BF16),
            pltpu.VMEM((CHUNK, width), BF16),
            pltpu.VMEM((q_rows + 2 * kv_rows, width), BF16),
            pltpu.VMEM((4 * width, channels), BF16),
            pltpu.VMEM((1024, channels), F32),
            pltpu.VMEM((width, pool_cols), BF16),
            pltpu.VMEM((q_rows + pool_cols, width), BF16),
            pltpu.VMEM((blocks, q_rows, WINDOW), BF16),
            pltpu.VMEM((blocks + 1, 2 * kv_rows, WINDOW), BF16),
            pltpu.VMEM((rows + WINDOW, pool_cols), BF16),
            pltpu.VMEM((4, WINDOW, 2 * WINDOW), BF16),
            pltpu.VMEM((blocks, 8, channels), F32),
            pltpu.VMEM((n_sp, 8, channels), F32),
            pltpu.VMEM((rows // 2, q_rows + pool_cols), BF16),
            pltpu.VMEM((tiles, rows // 2, COLS), BF16),
            pltpu.VMEM((tiles, rows // 2, COLS), BF16),
            pltpu.VMEM((tiles, rows // 2, COLS), BF16),
            dma((6,)),
            dma((chunks,)),
            dma((chunks,)),
            dma((chunks,)),
            dma((2,)),
            dma((2,)),
            dma((n_sp,)),
            dma((n_sp,)),
            dma((tiles,)),
            dma((tiles,)),
            dma((tiles,)),
        ],
        compiler_params=pltpu.CompilerParams(
            collective_id=0, has_side_effects=True, vmem_limit_bytes=60 * 1024 * 1024
        ),
    )(
        tokens[0],
        gain.reshape(1, width),
        flat(wq),
        flat(wk),
        flat(wv),
        sink,
        wp.reshape(-1, channels),
        wo.reshape(-1, width),
        wpo.reshape(-1, width),
    )
    return result[None]


def solution(mesh):
    in_specs = (
        P("fs", ("grp", "sp"), "tp"),
        P(),
        P(None, "tp", None),
        P(None, "tp", None),
        P(None, "tp", None),
        P("tp"),
        P(None, None, "tp"),
        P("tp", None, None),
        P(None, "tp", None),
    )
    out_specs = P("fs", ("grp", "sp", "tp"), None)
    return jax.shard_map(
        functools.partial(shards, mesh.shape["sp"]),
        mesh=mesh,
        in_specs=in_specs,
        out_specs=out_specs,
        check_vma=False,
    )
```

time: 104 us -> 29.1 us (0.28)
  matrix products: 30.6 us -> 0 us
  Pallas kernels: 0 us -> 26.1 us
  waiting for transfers between devices: 23.4 us -> 0 us
  between operations: 13.7 us -> 0.01 us
  other arithmetic: 12 us -> 0 us
  starting transfers between devices: 10.6 us -> 0 us
  blocking collectives: 6.44 us -> 0 us
  local copies, waits for them, and re-layouts: 6.9 us -> 2.73 us
    dot_general x8 -> x0, matrix products: 30.6 us -> none  [the longest x1 11.3 us: shards(): jnp.dot(pooled, pool_weight_rows, preferred_element_type=jnp.float32)]
    pallas_call x0 -> x1, Pallas kernels: none -> 26.1 us  [shards(): pl.pallas_call(functools.partial(kernel, n_sp, heads, local_kv, head_dim)...]
    reduce_scatter x1 -> x0, waiting for transfers between devices: 12.3 us -> none  [shards(): lax.psum_scatter((part_sum + jnp.dot(pooled, pool_weight_rows, preferred_...]
    ppermute x3 -> x0, starting transfers between devices: 10.6 us -> none  [from_behind(): lax.ppermute(value, axis, [(source, source + steps) for source in range(f...]
    all_gather x1 -> x0, waiting for transfers between devices: 10.4 us -> none  [shards(): whole = lax.all_gather(tokens, 'tp', axis=2, tiled=True)[0]]
    all_gather x1 -> x0, blocking collectives: 6.44 us -> none  [shards(): totals = lax.all_gather(prefix_total[None], 'sp', axis=0, tiled=True)]
    reduce_sum x4 -> x0, other arithmetic: 5.18 us -> none  [the longest x1 2.72 us: rms_norm(): scale = lax.rsqrt(jnp.mean(values * values, axis=-1, keepdims=True) + 1e-06)]
    reshape x5 -> x0, local copies, waits for them, and re-layouts: 4.17 us -> none  [the longest x1 3.63 us: attend(): qb = query.reshape(blocks, WINDOW, local_kv, group, head_dim)]
  transfers between devices with their start and end apart: 5 -> 0, of which waited for: 2 -> 0; matrix products, arithmetic and copies ran while one was open for 28% -> 0% of each run, Pallas kernels for 0% -> 0%
where the time goes in v1:
time: 29.1 us; the launch traced here: 28.8 us
  Pallas kernels  26.1 us (90%)
  local copies, waits for them, and re-layouts  2.73 us (9%)
    pallas_call x1, Pallas kernels, shards(): pl.pallas_call(functools.partial(kernel, n_sp, heads, local_kv, head_dim)...  26.1 us
    unnamed x1, local copies, waits for them, and re-layouts  2.73 us

profile of v1, /device:TPU:1, one launch (start us, length us, event | category | flops | bytes accessed | tf_op | source)
XLA Modules:
  0.0 28.8 jit_solution(12346352583286955275)
XLA Ops:
  0.0 26.1 %shard_map.91 = bf16[384,2048]{1,0:T(8,128)(2,1)} custom-call(bf16[768,1024]{1,0:T(8,128)(2,1)} %bitcast.20, f32[1,2048]{1,0:T(1,128)} %bitcast.23, bf16[512,2048]{1,0:T(8,128)(2,1)} %bitcast.16, bf16[128,2048]{1,0:T(8,128)(2,1)} %bitcast.21, bf16[128,2048]{1,0:T(8,128)(2,1)} %bitcast.22, f32[8]{0:T(128)} %sink.1, bf16[8192,128]{1,0:T(8,128)(2,1)} %bitcast.17, ...), custom_call_target="tpu_custom_call" | custom-call | tf_op jit(solution)/shard_map/pallas_call | solution.py:385
  26.1 2.7 %copy.11 = bf16[1,384,2048]{2,1,0:T(8,128)(2,1)} copy(bf16[1,384,2048]{2,1,0:T(8,128)(2,1)} %bitcast.15) | data formatting | bytes 3145728

commit v2 on v1

--- a/solution.py
+++ b/solution.py
@@ -52,7 +52,6 @@
     act,
     sending,
     landing,
-    result,
     w_sem,
     tok_sem,
     tok_send,
@@ -63,7 +62,7 @@
     tot_recv,
     out_send,
     out_recv,
-    out_sem,
+    entered,
 ):
     me_sp = lax.axis_index("sp")
     me_tp = lax.axis_index("tp")
@@ -82,14 +81,20 @@
     tiles = width // COLS
     group = heads // local_kv
 
+    for index in range(n_sp):
+        totals[index] = jnp.zeros((8, channels), F32)
     barrier = pltpu.get_barrier_semaphore()
     pl.semaphore_signal(barrier, inc=1, device_id={"tp": other}, device_id_type=MESH)
-    for step in range(1, n_sp):
-        peer = lax.rem(me_sp + step, n_sp)
-        pl.semaphore_signal(barrier, inc=1, device_id={"sp": peer}, device_id_type=MESH)
+
+    @pl.when(me_sp > 0)
+    def _():
+        pl.semaphore_signal(barrier, inc=1, device_id={"sp": me_sp - 1}, device_id_type=MESH)
+
+    @pl.when(me_sp < n_sp - 1)
+    def _():
+        pl.semaphore_signal(barrier, inc=1, device_id={"sp": me_sp + 1}, device_id_type=MESH)
 
     load_wp = pltpu.make_async_copy(wp, wp_raw, w_sem.at[0])
-    load_wp.start()
 
     def local_tokens(c):
         at = pl.ds(pl.multiple_of(c * CHUNK, CHUNK), CHUNK)
@@ -108,6 +113,7 @@
 
     for c in reversed(range(chunks)):
         local_tokens(c).start()
+    load_wp.start()
     loads = [
         pltpu.make_async_copy(wq, wqkv.at[pl.ds(0, q_rows), :], w_sem.at[1]),
         pltpu.make_async_copy(wk, wqkv.at[pl.ds(q_rows, kv_rows), :], w_sem.at[2]),
@@ -133,7 +139,8 @@
         ext[pl.ds(WINDOW - TAIL, TAIL), :] = jnp.zeros((TAIL, pool_cols), BF16)
         kvt[0] = jnp.zeros((2 * kv_rows, WINDOW), BF16)
 
-    pl.semaphore_wait(barrier, n_sp)
+    neighbours = jnp.where(me_sp > 0, 1, 0) + jnp.where(me_sp < n_sp - 1, 1, 0)
+    pl.semaphore_wait(barrier, 1 + neighbours)
     for c in reversed(range(chunks)):
         remote_tokens(c).start()
     for load in load_out:
@@ -174,8 +181,7 @@
 
     scale = head_dim ** (-0.5)
 
-    def project(i, carry):
-        c = chunks - 1 - i
+    def normalize(c):
         local_tokens(c).wait()
         remote_tokens(c).wait_recv()
         at = pl.ds(pl.multiple_of(c * CHUNK, CHUNK), CHUNK)
@@ -184,49 +190,89 @@
         square = jnp.sum(low * low, axis=1, keepdims=True)
         square = square + jnp.sum(high * high, axis=1, keepdims=True)
         inv = lax.rsqrt(square * (1.0 / width) + 1e-06)
-        normed[:, pl.ds(0, half_width)] = (low * inv * gain[:, pl.ds(0, half_width)]).astype(BF16)
-        normed[:, pl.ds(half_width, half_width)] = (
+        normed[c, :, pl.ds(0, half_width)] = (low * inv * gain[:, pl.ds(0, half_width)]).astype(
+            BF16
+        )
+        normed[c, :, pl.ds(half_width, half_width)] = (
             high * inv * gain[:, pl.ds(half_width, half_width)]
         ).astype(BF16)
 
-        @pl.when((i == 1) & (me_sp < n_sp - 1))
-        def _():
-            halo_kv.start()
-            halo_pool.start()
-
-        pooled_in = dot(normed[...], wpool[...]).astype(BF16)
+    def project_pool(c):
+        pooled_in = dot(normed[c], wpool[...]).astype(BF16)
         ext[pl.ds(pl.multiple_of(WINDOW + c * CHUNK, WINDOW), CHUNK), :] = pooled_in
         last = pooled_in[:, 3 * channels :].astype(F32)
         for j in range(per_chunk):
             summed = jnp.sum(last[j * WINDOW : (j + 1) * WINDOW], axis=0, keepdims=True)
             block_sum[c * per_chunk + j] = jnp.broadcast_to(summed, (8, channels))
-        qkv = dot(wqkv[...], normed[...], ((1,), (1,)))
+
+    def project_qkv(c):
+        qkv = dot(wqkv[...], normed[c], ((1,), (1,)))
         for j in range(per_chunk):
             b = c * per_chunk + j
             piece = qkv[:, j * WINDOW : (j + 1) * WINDOW]
             qt[b] = (piece[:q_rows] * scale).astype(BF16)
             kvt[b + 1] = piece[q_rows:].astype(BF16)
+
+    def hear(step):
+        @pl.when(me_sp + step < n_sp - 1)
+        def _():
+            pl.semaphore_wait(entered.at[step], 1)
+
+    def tell(step):
+        @pl.when((me_sp > 0) & (me_sp + step - 1 < n_sp - 1))
+        def _():
+            pl.semaphore_signal(
+                entered.at[step], inc=1, device_id={"sp": me_sp - 1}, device_id_type=MESH
+            )
+
+    if n_sp > 2:
+        tell(1)
+
+    def project(i, carry):
+        c = chunks - 1 - i
+        normalize(c)
+
+        @pl.when((i == 1) & (me_sp < n_sp - 1))
+        def _():
+            halo_kv.start()
+            halo_pool.start()
+
+        @pl.when(i > 0)
+        def _():
+            hear(i)
+            tell(i + 1)
+
+        project_pool(c)
+        project_qkv(c)
         return carry
 
     lax.fori_loop(0, chunks, project, 0)
+
+    for step in range(chunks, n_sp - 1):
+        hear(step)
+        if step < n_sp - 2:
+            tell(step + 1)
 
     all_rows = block_sum[0]
     for b in range(1, blocks):
         all_rows = all_rows + block_sum[b]
     totals[me_sp] = all_rows
-    sends = []
+
+    def total_copy(step):
+        return pltpu.make_async_remote_copy(
+            src_ref=totals.at[me_sp],
+            dst_ref=totals.at[me_sp],
+            send_sem=tot_send.at[step],
+            recv_sem=tot_recv.at[step],
+            device_id={"sp": lax.rem(me_sp + step, n_sp)},
+            device_id_type=MESH,
+        )
+
     for step in range(1, n_sp):
-        peer = lax.rem(me_sp + step, n_sp)
-        sends.append(
-            pltpu.make_async_remote_copy(
-                src_ref=totals.at[me_sp],
-                dst_ref=totals.at[me_sp],
-                send_sem=tot_send.at[step],
-                recv_sem=tot_recv.at[step],
-                device_id={"sp": peer},
-                device_id_type=MESH,
-            )
-        )
+
+        @pl.when(me_sp + step < n_sp)
+        def _():
+            total_copy(step).start()
 
     key_at = lax.broadcasted_iota(jnp.int32, (WINDOW, group * WINDOW), 0)
     query_at = lax.rem(
@@ -286,9 +332,6 @@
             pooled = sums * (1.0 / denom) - own.astype(F32)
             act[at, pl.ds(q_rows + g * channels, channels)] = pooled.astype(BF16)
 
-    for send in sends:
-        send.start()
-
     @pl.when(me_sp > 0)
     def _():
         halo_kv.wait_recv()
@@ -299,19 +342,23 @@
             attend(first + i, i)
             return carry
 
-        lax.fori_loop(0, half_blocks, one, 0)
+        lax.fori_loop(0, half_blocks, one, 0, unroll=True)
 
     def pool_half(first, carried):
         def one(i, carry):
             pool(first + i, i, carried)
             return carry
 
-        lax.fori_loop(0, half_blocks, one, 0)
+        lax.fori_loop(0, half_blocks, one, 0, unroll=True)
 
     first = other * half_blocks
     attend_half(first)
-    for send in sends:
-        send.wait()
+    for step in range(1, n_sp):
+
+        @pl.when(me_sp - step >= 0)
+        def _():
+            total_copy(step).wait_recv()
+
     carried = jnp.zeros((8, channels), F32)
     for index in range(n_sp):
         carried = carried + jnp.where(index < me_sp, totals[index], 0.0)
@@ -343,22 +390,23 @@
     attend_half(first)
     pool_half(first, carried)
 
-    def store(t):
-        return pltpu.make_async_copy(result.at[t], out.at[:, columns(t)], out_sem.at[t])
-
     def keep(t, carry):
         partial_send(t).wait_recv()
         mine = dot(act[...], wout[:, columns(t)])
-        result[t] = (mine + landing[t].astype(F32)).astype(BF16)
-        store(t).start()
+        out[:, columns(t)] = (mine + landing[t].astype(F32)).astype(BF16)
         return carry
 
     lax.fori_loop(0, tiles, keep, 0)
     for t in range(tiles):
-        store(t).wait()
         partial_send(t).wait_send()
     for c in range(chunks):
         remote_tokens(c).wait_send()
+    for step in range(1, n_sp):
+
+        @pl.when(me_sp + step < n_sp)
+        def _():
+            total_copy(step).wait_send()
+
 
     @pl.when(me_sp < n_sp - 1)
     def _():
@@ -379,17 +427,17 @@
     chunks = rows // CHUNK
     dma = pltpu.SemaphoreType.DMA
     flat = lambda w: jnp.transpose(w, (1, 2, 0)).reshape(-1, width)
-    hbm = pl.BlockSpec(memory_space=pl.ANY)
+    hbm = pl.BlockSpec(memory_space=pltpu.HBM)
     vmem = pl.BlockSpec(memory_space=pltpu.VMEM)
     smem = pl.BlockSpec(memory_space=pltpu.SMEM)
     result = pl.pallas_call(
         functools.partial(kernel, n_sp, heads, local_kv, head_dim),
-        out_shape=jax.ShapeDtypeStruct((rows // 2, width), BF16),
+        out_shape=pltpu.VMEM((rows // 2, width), BF16),
         in_specs=[hbm, vmem, hbm, hbm, hbm, smem, hbm, hbm, hbm],
-        out_specs=hbm,
+        out_specs=vmem,
         scratch_shapes=[
             pltpu.VMEM((2, rows, half_width), BF16),
-            pltpu.VMEM((CHUNK, width), BF16),
+            pltpu.VMEM((chunks, CHUNK, width), BF16),
             pltpu.VMEM((q_rows + 2 * kv_rows, width), BF16),
             pltpu.VMEM((4 * width, channels), BF16),
             pltpu.VMEM((1024, channels), F32),
@@ -404,7 +452,6 @@
             pltpu.VMEM((rows // 2, q_rows + pool_cols), BF16),
             pltpu.VMEM((tiles, rows // 2, COLS), BF16),
             pltpu.VMEM((tiles, rows // 2, COLS), BF16),
-            pltpu.VMEM((tiles, rows // 2, COLS), BF16),
             dma((6,)),
             dma((chunks,)),
             dma((chunks,)),
@@ -415,10 +462,10 @@
             dma((n_sp,)),
             dma((tiles,)),
             dma((tiles,)),
-            dma((tiles,)),
+            pltpu.SemaphoreType.REGULAR((n_sp,)),
         ],
         compiler_params=pltpu.CompilerParams(
-            collective_id=0, has_side_effects=True, vmem_limit_bytes=60 * 1024 * 1024
+            collective_id=0, has_side_effects=True, vmem_limit_bytes=67043328 - rows * width - 65536
         ),
     )(
         tokens[0],

time: 29.1 us -> 22.5 us (0.77)
  Pallas kernels: 26.1 us -> 21.2 us
  local copies, waits for them, and re-layouts: 2.73 us -> 1.15 us
    pallas_call x1, Pallas kernels: 26.1 us -> 21.2 us  [shards(): pl.pallas_call(functools.partial(kernel, n_sp, heads, local_kv, head_dim)...]
    unnamed x1, local copies, waits for them, and re-layouts: 2.73 us -> 1.15 us
where the time goes in v2:
time: 22.5 us; the launch traced here: 22.3 us
  Pallas kernels  21.2 us (94%)
  local copies, waits for them, and re-layouts  1.15 us (5%)
    pallas_call x1, Pallas kernels, shards(): pl.pallas_call(functools.partial(kernel, n_sp, heads, local_kv, head_dim)...  21.2 us
    unnamed x1, local copies, waits for them, and re-layouts  1.15 us

profile of v2, /device:TPU:1, one launch (start us, length us, event | category | flops | bytes accessed | tf_op | source)
XLA Modules:
  0.0 22.3 jit_solution(11835376838824834636)
XLA Ops:
  0.0 21.2 %shard_map.91 = bf16[384,2048]{1,0:T(8,128)(2,1)S(1)} custom-call(bf16[768,1024]{1,0:T(8,128)(2,1)} %bitcast.20, f32[1,2048]{1,0:T(1,128)} %bitcast.23, bf16[512,2048]{1,0:T(8,128)(2,1)} %bitcast.16, bf16[128,2048]{1,0:T(8,128)(2,1)} %bitcast.21, bf16[128,2048]{1,0:T(8,128)(2,1)} %bitcast.22, f32[8]{0:T(128)} %sink.1, bf16[8192,128]{1,0:T(8,128)(2,1)} %bitcast.17, ...), custom_call_target="tpu_custom_call" | custom-call | tf_op jit(solution)/shard_map/pallas_call | solution.py:433
  21.2 1.1 %copy.11 = bf16[1,384,2048]{2,1,0:T(8,128)(2,1)} copy(bf16[1,384,2048]{2,1,0:T(8,128)(2,1)S(1)} %bitcast.15) | data formatting | bytes 3145728
